TPU v7x, 32 devices: a whole 2x2x4 slice. The times are simulated.
32 devices in a mesh: grp: 2 (over y), sp: 4 (over z), tp: 4 (over x, core).
Axes of the slice: x: 2, y: 2, z: 4, core: 2. Of those that a mesh axis runs over, the one named last changes fastest.
Arguments:
- query_rows: bfloat16 [4096, 1024], P(('grp', 'sp'), 'tp'), parts along dimension 0, may hold values from -128 to 128
- key_rows: bfloat16 [4096, 256], P(('grp', 'sp'), 'tp'), parts along dimension 0, may hold values from -4 to 4
- value_rows: bfloat16 [4096, 256], P(('grp', 'sp'), 'tp'), parts along dimension 0, may hold values from -6 to 6
- sink_logits: float32 [16], P('tp'), may hold values from 3 to 7
- residual: bfloat16 [4096, 2048], P(('grp', 'sp', 'tp')), parts along dimension 0, may hold values from -6 to 6
- out_weight: bfloat16 [1024, 2048], P('tp'), may hold values from -0.1875 to 0.1875
- norm_gain: float32 [2048], replicated, may hold values from 0.1 to 1.9
- gate_weight: bfloat16 [16, 2048, 512], P(('sp', 'tp')), may hold values from -0.125 to 0.125
- up_weight: bfloat16 [16, 2048, 512], P(('sp', 'tp')), may hold values from -0.125 to 0.125
- down_weight: bfloat16 [16, 512, 2048], P(('sp', 'tp')), may hold values from -0.25 to 0.25
- routes: int32 [4096, 2], P(('grp', 'sp', 'tp')), parts along dimension 0, may hold values from 0 to 15, as said below
- route_weight: float32 [4096, 2], P(('grp', 'sp', 'tp')), parts along dimension 0, may hold values from 0.1 to 1
Outputs:
- layer_out: bfloat16 [4096, 2048], P(('grp', 'sp', 'tp')), parts along dimension 0
There are 2 independent parts, one for each index of `grp`. A program takes and returns all parts, laid end to end along the dimension named above; an argument that names none is the same for every part. Nothing has to cross between parts.
Inputs may be any that keep to these rules, and one draw needn't show every extreme that they name: `routes`: A token's two experts differ and lie in the same group of 4 consecutive experts. Among the 128 tokens of one device (aligned blocks of 128 rows) no expert is named more than 32 times; in every block each expert of one group, the same group for all blocks, is named exactly 32 times.
All inputs are finite; a program needn't handle non-finite values.
Results may differ from a plain program's by a relative error of at most 0.013.
Values may be sent and summed in bfloat16 or wider, within the bound.
No kernel may reach another device: no remote copies, remote signals or barrier semaphores. Data moves between devices by JAX's collectives and lax.ppermute only.
A program may use at most 64 MiB of HBM per device.

v0:
```python
import jax
import jax.numpy as jnp
from jax import lax
from jax.sharding import PartitionSpec as P

HDIM = 64
WINDOW = 128
rope_base = 10000.0
norm_eps = 1e-06


def shifted(block, axis, distance):
    devices = range(lax.axis_size(axis))
    route = [(i - distance, i) for i in devices if i - distance in devices]
    return lax.ppermute(block, axis, route)


def rotate(rows, positions, heads):
    half_dim = HDIM // 2
    values = rows.astype(jnp.float32).reshape(rows.shape[0], heads, HDIM)
    inverse = rope_base ** (-jnp.arange(half_dim, dtype=jnp.float32) / half_dim)
    angles = positions.astype(jnp.float32)[:, None] * inverse[None, :]
    cosines = jnp.cos(angles)[:, None, :]
    sines = jnp.sin(angles)[:, None, :]
    lower = values[..., :half_dim]
    upper = values[..., half_dim:]
    turned = jnp.concatenate(
        [lower * cosines - upper * sines, upper * cosines + lower * sines], axis=-1
    )
    return turned.reshape(rows.shape[0], heads * HDIM).astype(jnp.bfloat16)


def per_device(
    query_rows,
    key_rows,
    value_rows,
    sink_logits,
    residual,
    out_weight,
    norm_gain,
    gate_weight,
    up_weight,
    down_weight,
    routes,
    route_weight,
):
    tok_count = query_rows.shape[0]
    head_local = query_rows.shape[1] // HDIM
    group_local = key_rows.shape[1] // HDIM
    repeat = head_local // group_local
    first_pos = lax.axis_index("sp") * tok_count
    positions = first_pos + jnp.arange(tok_count, dtype=jnp.int32)
    rot_q = rotate(query_rows, positions, head_local)
    rot_k = rotate(key_rows, positions, group_local)
    tails = jnp.stack([rot_k[tok_count - WINDOW :], value_rows[tok_count - WINDOW :]])
    earlier = shifted(tails, "sp", 1)
    blocks = tok_count // WINDOW
    q_blocks = rot_q.reshape(blocks, WINDOW, group_local, repeat, HDIM)
    k_blocks = rot_k.reshape(blocks, WINDOW, group_local, HDIM)
    v_blocks = value_rows.reshape(blocks, WINDOW, group_local, HDIM)
    k_prev = jnp.concatenate(
        [earlier[0].reshape(1, WINDOW, group_local, HDIM), k_blocks[:-1]], axis=0
    )
    v_prev = jnp.concatenate(
        [earlier[1].reshape(1, WINDOW, group_local, HDIM), v_blocks[:-1]], axis=0
    )
    k_wide = jnp.concatenate([k_prev, k_blocks], axis=1)
    v_wide = jnp.concatenate([v_prev, v_blocks], axis=1)
    query_pos = jnp.arange(WINDOW) + WINDOW
    key_pos = jnp.arange(2 * WINDOW)
    distance = query_pos[:, None] - key_pos[None, :]
    in_band = (distance >= 0) & (distance < WINDOW)
    key_global = (
        first_pos + jnp.arange(blocks)[:, None, None] * WINDOW + key_pos[None, None, :] - WINDOW
    )
    allowed = in_band[None] & (key_global >= 0)
    scores = jnp.einsum(
        "nqgrd,nkgd->grnqk", q_blocks, k_wide, preferred_element_type=jnp.float32
    ) * HDIM ** (-0.5)
    scores = jnp.where(allowed[None, None], scores, -jnp.inf)
    sink_here = sink_logits.reshape(group_local, repeat)[:, :, None, None, None]
    largest = jnp.maximum(scores.max(axis=-1, keepdims=True), sink_here)
    exp_scores = jnp.exp(scores - largest)
    denominator = exp_scores.sum(axis=-1, keepdims=True) + jnp.exp(sink_here - largest)
    probs = (exp_scores / denominator).astype(jnp.bfloat16)
    attended = jnp.einsum("grnqk,nkgd->nqgrd", probs, v_wide, preferred_element_type=jnp.float32)
    attended = attended.astype(jnp.bfloat16).reshape(tok_count, head_local * HDIM)
    row_count = residual.shape[0]
    token_rows = lax.all_to_all(attended, "tp", split_axis=0, concat_axis=1, tiled=True)
    projected = jnp.dot(
        token_rows,
        lax.all_gather(out_weight, "tp", axis=0, tiled=True),
        preferred_element_type=jnp.float32,
    )
    stream_f = (residual.astype(jnp.float32) + projected).astype(jnp.bfloat16).astype(jnp.float32)
    normed = (
        stream_f
        * lax.rsqrt(jnp.mean(stream_f * stream_f, axis=-1, keepdims=True) + norm_eps)
        * norm_gain[None, :]
    ).astype(jnp.bfloat16)
    sp_count = lax.axis_size("sp")
    tp_count = lax.axis_size("tp")
    expert_count = sp_count * tp_count
    capacity = 4 * row_count // expert_count
    width = normed.shape[1]
    flat_expert = routes.reshape(-1)
    one_hot = (flat_expert[:, None] == jnp.arange(expert_count, dtype=jnp.int32)[None, :]).astype(
        jnp.int32
    )
    slot_rank = jnp.sum((jnp.cumsum(one_hot, axis=0) - one_hot) * one_hot, axis=1)
    slot_index = flat_expert * capacity + slot_rank
    token_of = jnp.arange(2 * row_count, dtype=jnp.int32) // 2
    outgoing = (
        jnp.zeros((expert_count * capacity, width), jnp.bfloat16)
        .at[slot_index]
        .set(normed[token_of])
    )
    outgoing = outgoing.reshape(expert_count, capacity, width)
    arrived = lax.all_to_all(outgoing, ("sp", "tp"), split_axis=0, concat_axis=0, tiled=True)
    flat_rows = arrived.reshape(-1, width)
    gate_out = jnp.dot(flat_rows, gate_weight[0], preferred_element_type=jnp.float32)
    up_out = jnp.dot(flat_rows, up_weight[0], preferred_element_type=jnp.float32)
    hidden = (jax.nn.silu(gate_out) * up_out).astype(jnp.bfloat16)
    produced = jnp.dot(hidden, down_weight[0], preferred_element_type=jnp.float32).astype(
        jnp.bfloat16
    )
    returned = lax.all_to_all(
        produced.reshape(arrived.shape), ("sp", "tp"), split_axis=0, concat_axis=0, tiled=True
    )
    gathered = returned.reshape(expert_count * capacity, width)[slot_index].astype(jnp.float32)
    weighted = gathered * route_weight.reshape(-1)[:, None]
    combined = weighted.reshape(row_count, 2, width).sum(axis=1)
    return (stream_f + combined).astype(jnp.bfloat16)


def solution(mesh):
    in_specs = (
        P(("grp", "sp"), "tp"),
        P(("grp", "sp"), "tp"),
        P(("grp", "sp"), "tp"),
        P("tp"),
        P(("grp", "sp", "tp"), None),
        P("tp", None),
        P(),
        P(("sp", "tp"), None, None),
        P(("sp", "tp"), None, None),
        P(("sp", "tp"), None, None),
        P(("grp", "sp", "tp"), None),
        P(("grp", "sp", "tp"), None),
    )
    out_specs = P(("grp", "sp", "tp"), None)
    return jax.shard_map(
        per_device, mesh=mesh, in_specs=in_specs, out_specs=out_specs, check_vma=False
    )
```

profile of v0, /device:TPU:11, one launch (start us, length us, event | category | flops | bytes accessed | tf_op | source)
XLA Modules:
  0.0 195.3 jit_solution(5464959872850920019)
XLA Ops:
  6.5 0.0 copy-start
  6.5 0.0 copy-start.5
  6.5 0.0 copy-start.2
  6.5 0.0 all-gather.2.cloned.1.call-start
  6.5 0.7 all-gather.2.cloned.1.call-update
  7.3 0.0 copy-start.3
  7.3 0.0 slice-start
  7.3 0.9 bitcast_convert_fusion
  8.2 0.3 fusion.38
  8.5 0.7 slice_bitcast_fusion.4
  9.3 3.2 %collective-permute-start = (bf16[2,128,64]{1,2,0:T(8,128)(2,1)S(1)}, bf16[2,128,64]{1,2,0:T(8,128)(2,1)S(1)}, u32[]{:S(2)}, u32[]{:S(2)}) collective-permute-start(bf16[2,128,64]{1,2,0:T(8,128)(2,1)S(1)} %pad_maximum_fusion), channel_id=1, source_target_pairs={{0,4},{4,8},{8,12},{1,5},{5,9},{9,13},{2,6},{6,10},{10,14},{3,7},{... | collective-permute-start | bytes 98312 | tf_op jit(solution)/shard_map/ppermute | solution.py:15
  12.5 0.8 copy.25
  13.2 0.1 eq.29
  13.4 0.1 eq.25
  13.5 0.0 copy-done.2
  13.5 0.1 copy.21
  13.7 0.1 convert.12
  13.8 0.6 reduce-window.6
  14.3 0.2 slice_reduce_fusion
  14.6 0.1 fusion.42
  14.7 0.1 add_compare_fusion
  14.8 0.0 copy-done.5
  14.8 0.3 multiply_cosine_fusion
  15.2 0.2 broadcast_and_fusion
  15.4 0.1 subtract_convert_fusion
  15.5 0.0 copy-start.6
  15.5 0.0 copy-done.3
  15.5 0.0 slice-done
  15.6 0.1 copy.24
  15.7 0.1 mul.180
  15.8 0.0 collective-permute-done
  15.9 0.5 fusion.47
  16.4 0.0 copy-done.6
  16.4 0.1 broadcast_maximum_fusion
  16.5 0.3 fusion.7
  16.8 0.1 exponential_add_fusion
  16.9 1.2 convolution_convert_fusion.1
  18.1 4.5 %all-to-all-start = ((bf16[4,128,256]{1,2,0:T(8,128)(2,1)}), bf16[4,128,256]{1,2,0:T(8,128)(2,1)S(1)}, u32[]{:S(2)}, u32[]{:S(2)}) async-start(bf16[4,128,256]{1,2,0:T(8,128)(2,1)} %bitcast.20), calls=%async_computation | async-start | bytes 524288 | tf_op jit(solution)/shard_map/all_to_all | solution.py:89
  22.5 7.4 %all-to-all-done = bf16[4,128,256]{1,2,0:T(8,128)(2,1)S(1)} async-done(((bf16[4,128,256]{1,2,0:T(8,128)(2,1)}), bf16[4,128,256]{1,2,0:T(8,128)(2,1)S(1)}, u32[]{:S(2)}, u32[]{:S(2)}) %all-to-all-start) | async-done | bytes 262176 | tf_op jit(solution)/shard_map/all_to_all | solution.py:89
  29.9 16.9 %all-gather.2.cloned.1.call-done = bf16[1024,2048]{1,0:T(8,128)(2,1)} async-done(((bf16[256,2048]{1,0:T(8,128)(2,1)}), bf16[1024,2048]{1,0:T(8,128)(2,1)}) %all-gather.2.cloned.1.call-update) | async-done | bytes 4194320 | tf_op jit(solution)/shard_map/all_gather | solution.py:92
  46.9 0.0 copy-start.4
  46.9 3.1 %multiply_reduce_fusion.1 = (f32[128]{0:T(128)S(1)}, f32[128,2048]{1,0:T(8,128)S(1)}) fusion(bf16[128,1024]{0,1:T(8,128)(2,1)S(1)} %bitcast.116, bf16[1024,2048]{1,0:T(8,128)(2,1)} %all-gather.2.cloned.1.call-done, bf16[128,2048]{1,0:T(8,128)(2,1)} %param.16), kind=kOutput, calls=%fused_computation.25 | convolution fusion | flops 538443648 | bytes 6029824 | tf_op jit(solution)/shard_map/dot_general | solution.py:90
  50.0 0.0 copy-done.4
  50.0 1.0 multiply_convert_fusion
  51.0 7.3 %scatter_custom_fusion = bf16[512,2048]{1,0:T(8,128)(2,1)} fusion(s32[256]{0:T(256)S(1)} %bitcast.119, bf16[128,2048]{1,0:T(8,128)(2,1)} %multiply_convert_fusion, s32[1024]{0:T(1024)S(1)} %pad_clamp_fusion.1, bf16[]{:T(256)} %constant.56.clone.1), kind=kCustom, calls=%fused_computation.21 | custom fusion | bytes 2097664 | tf_op jit(solution)/shard_map/scatter | solution.py:116
  58.3 0.0 copy-start.8
  58.3 53.3 %all_to_all.29 = bf16[16,32,2048]{2,1,0:T(8,128)(2,1)S(1)} all-to-all(bf16[16,32,2048]{2,1,0:T(8,128)(2,1)} %bitcast.112), channel_id=1, replica_groups=mesh['grp'=2,'sp'=4,'tp'=4] {'sp','tp'}, dimensions={0} | all-to-all | bytes 4194304 | tf_op jit(solution)/shard_map/all_to_all | solution.py:119
  111.6 0.0 copy-start.1
  111.7 1.3 copy-done.1
  112.9 0.0 copy-done.8
  112.9 2.2 %fusion.5 = f32[512,512]{1,0:T(8,128)} fusion(bf16[512,2048]{1,0:T(8,128)(2,1)S(1)} %bitcast.114, bf16[1,2048,512]{2,1,0:T(8,128)(2,1)S(1)} %copy-done.8), kind=kOutput, calls=%fused_computation.11 | convolution fusion | flops 1073741824 | bytes 5242880 | tf_op jit(solution)/shard_map/dot_general | solution.py:121
  115.2 0.0 copy-done
  115.2 6.3 %convolution_convert_fusion = bf16[512,2048]{1,0:T(8,128)(2,1)} fusion(bf16[1,512,2048]{2,1,0:T(8,128)(2,1)S(1)} %copy-done, bf16[512,2048]{1,0:T(8,128)(2,1)} %bitcast.115, bf16[1,2048,512]{2,1,0:T(8,128)(2,1)} %param.20, f32[512,512]{1,0:T(8,128)} %fusion.5), kind=kOutput, calls=%fused_computation.3 | convolution fusion | flops 2150105088 | bytes 9437184 | tf_op jit(solution)/shard_map/dot_general | solution.py:124
  121.5 0.0 copy-start.7
  121.5 5.1 %all-to-all-start.2 = ((bf16[16,32,2048]{2,1,0:T(8,128)(2,1)}), bf16[16,32,2048]{2,1,0:T(8,128)(2,1)}, u32[]{:S(2)}, u32[]{:S(2)}) async-start(bf16[16,32,2048]{2,1,0:T(8,128)(2,1)} %bitcast.113), calls=%async_computation.2 | async-start | bytes 4194304 | tf_op jit(solution)/shard_map/all_to_all | solution.py:127
  126.6 0.0 copy-done.7
  126.6 0.1 copy.28
  126.7 47.4 %all-to-all-done.2 = bf16[16,32,2048]{2,1,0:T(8,128)(2,1)} async-done(((bf16[16,32,2048]{2,1,0:T(8,128)(2,1)}), bf16[16,32,2048]{2,1,0:T(8,128)(2,1)}, u32[]{:S(2)}, u32[]{:S(2)}) %all-to-all-start.2) | async-done | bytes 2097184 | tf_op jit(solution)/shard_map/all_to_all | solution.py:127
  174.1 5.2 %gather_fusion = bf16[256,2048]{1,0:T(8,128)(2,1)} fusion(bf16[512,2048]{1,0:T(8,128)(2,1)} %bitcast.33, s32[1024]{0:T(1024)S(1)} %pad_clamp_fusion), kind=kCustom, calls=%fused_computation.1 | custom fusion | bytes 2098176 | tf_op jit(solution)/shard_map/gather | solution.py:130
  179.3 3.4 %reshape.391 = f32[128,2,2048]{2,1,0:T(2,128)} reshape(bf16[256,2048]{1,0:T(8,128)(2,1)} %gather_fusion) | data formatting | bytes 3145728 | tf_op jit(solution)/shard_map/convert_element_type | solution.py:130
  182.7 4.8 %multiply_reduce_fusion = f32[128,2048]{1,0:T(8,128)S(1)} fusion(f32[128,2,2048]{2,1,0:T(2,128)} %reshape.391, f32[128,2]{1,0:T(8,128)S(1)} %copy.28), kind=kLoop, calls=%fused_computation.13 | loop fusion | flops 786432 | bytes 3146752 | tf_op jit(solution)/shard_map/reduce_sum | solution.py:132
  187.5 0.9 add_convert_fusion
  (24 shorter events, 0.3 us)
Async XLA Ops:
  6.5 108.6 %copy-start = (bf16[1,512,2048]{2,1,0:T(8,128)(2,1)S(1)}, bf16[1,512,2048]{2,1,0:T(8,128)(2,1)}, u32[]{:S(2)}) copy-start(bf16[1,512,2048]{2,1,0:T(8,128)(2,1)} %param.21) | copy-start | bytes 6291460
  6.5 8.2 %copy-start.5 = (s32[128,2]{0,1:T(2,128)S(1)}, s32[128,2]{0,1:T(2,128)}, u32[]{:S(2)}) copy-start(s32[128,2]{0,1:T(2,128)} %param.22) | copy-start | bytes 3076
  6.5 7.0 %copy-start.2 = (bf16[512,256]{1,0:T(8,128)(2,1)S(1)}, bf16[512,256]{1,0:T(8,128)(2,1)}, u32[]{:S(2)}) copy-start(bf16[512,256]{1,0:T(8,128)(2,1)} %param.12) | copy-start | bytes 786436
  6.5 40.3 %all-gather.2.cloned.1.call-start = ((), (), s32[]{:S(2)}) async-start(), calls=%async_computation.3 | async-start | bytes 5242880 | tf_op jit(solution)/shard_map/all_gather | solution.py:92
  7.3 8.2 %copy-start.3 = (bf16[512,64]{0,1:T(8,128)(2,1)S(1)}, bf16[512,64]{0,1:T(8,128)(2,1)}, u32[]{:S(2)}) copy-start(bf16[512,64]{0,1:T(8,128)(2,1)} %param.14) | copy-start | bytes 196612
  7.3 8.2 %slice-start = ((bf16[512,64]{0,1:T(8,128)(2,1)}), bf16[384,64]{0,1:T(8,128)(2,1)S(1)}, s32[]{:S(2)}) async-start(bf16[512,64]{0,1:T(8,128)(2,1)} %param.14), calls=%async_computation.4 | async-start | bytes 98304 | tf_op jit(solution)/shard_map/slice | solution.py:65
  9.3 6.6 %collective-permute-start = (bf16[2,128,64]{1,2,0:T(8,128)(2,1)S(1)}, bf16[2,128,64]{1,2,0:T(8,128)(2,1)S(1)}, u32[]{:S(2)}, u32[]{:S(2)}) collective-permute-start(bf16[2,128,64]{1,2,0:T(8,128)(2,1)S(1)} %pad_maximum_fusion), channel_id=1, source_target_pairs={{0,4},{4,8},{8,12},{1,5},{5,9},{9,13},{2,6},{6,10},{10,14},{3,7},{... | collective-permute-start | bytes 98312 | tf_op jit(solution)/shard_map/ppermute | solution.py:15
  15.5 0.9 copy-start.6
  18.1 11.8 %all-to-all-start = ((bf16[4,128,256]{1,2,0:T(8,128)(2,1)}), bf16[4,128,256]{1,2,0:T(8,128)(2,1)S(1)}, u32[]{:S(2)}, u32[]{:S(2)}) async-start(bf16[4,128,256]{1,2,0:T(8,128)(2,1)} %bitcast.20), calls=%async_computation | async-start | bytes 524288 | tf_op jit(solution)/shard_map/all_to_all | solution.py:89
  46.9 3.2 %copy-start.4 = (f32[2048]{0:T(1024)S(1)}, f32[2048]{0:T(1024)}, u32[]{:S(2)}) copy-start(f32[2048]{0:T(1024)} %param.18) | copy-start | bytes 24580
  58.3 54.6 %copy-start.8 = (bf16[1,2048,512]{2,1,0:T(8,128)(2,1)S(1)}, bf16[1,2048,512]{2,1,0:T(8,128)(2,1)}, u32[]{:S(2)}) copy-start(bf16[1,2048,512]{2,1,0:T(8,128)(2,1)} %param.19) | copy-start | bytes 6291460
  111.6 1.3 copy-start.1
  121.5 5.1 %copy-start.7 = (f32[128,2]{0,1:T(2,128)S(1)}, f32[128,2]{0,1:T(2,128)}, u32[]{:S(2)}) copy-start(f32[128,2]{0,1:T(2,128)} %param.23) | copy-start | bytes 3076
  121.5 52.7 %all-to-all-start.2 = ((bf16[16,32,2048]{2,1,0:T(8,128)(2,1)}), bf16[16,32,2048]{2,1,0:T(8,128)(2,1)}, u32[]{:S(2)}, u32[]{:S(2)}) async-start(bf16[16,32,2048]{2,1,0:T(8,128)(2,1)} %bitcast.113), calls=%async_computation.2 | async-start | bytes 4194304 | tf_op jit(solution)/shard_map/all_to_all | solution.py:127
Sparse Core Ops, SparseCore 0:
  8.9 37.9 all-gather.1
where the time goes:
time: 196 us; the launch traced here: 195 us
  waiting for transfers between devices  72.4 us (37%)
  blocking collectives  53.3 us (27%)
  local copies, waits for them, and re-layouts  19.8 us (10%)
  between operations  13.7 us (7%)
  matrix products  13.4 us (7%)
  starting transfers between devices  12.8 us (7%)
  other arithmetic  9.91 us (5%)
    all_to_all x1, blocking collectives, per_device(): lax.all_to_all(outgoing, ('sp', 'tp'), split_axis=0, concat_axis=0, tiled...  53.3 us
    all_to_all x1, waiting for transfers between devices, per_device(): lax.all_to_all(produced.reshape(arrived.shape), ('sp', 'tp'), split_axis=...  47.4 us
    all_gather x1, waiting for transfers between devices, per_device(): lax.all_gather(out_weight, 'tp', axis=0, tiled=True)  16.9 us
    all_to_all x1, waiting for transfers between devices, per_device(): lax.all_to_all(attended, 'tp', split_axis=0, concat_axis=1, tiled=True)  7.37 us
    scatter x1, local copies, waits for them, and re-layouts, per_device(): outgoing = jnp.zeros((expert_count * capacity, width), jnp.bfloat16).at[s...  7.33 us
    dot_general x1, matrix products, per_device(): jnp.dot(hidden, down_weight[0], preferred_element_type=jnp.float32)  6.28 us
    gather x1, local copies, waits for them, and re-layouts, per_device(): returned.reshape(expert_count * capacity, width)[slot_index]  5.2 us
    all_to_all x1, starting transfers between devices, per_device(): lax.all_to_all(produced.reshape(arrived.shape), ('sp', 'tp'), split_axis=...  5.14 us
  transfers between devices with their start and end apart: 4, of which 3 were waited for; matrix products, arithmetic and copies ran while one was open for 4% of the time, Pallas kernels for 0%

commit v1 on v0

--- a/solution.py
+++ b/solution.py
@@ -86,7 +86,10 @@
     attended = jnp.einsum("grnqk,nkgd->nqgrd", probs, v_wide, preferred_element_type=jnp.float32)
     attended = attended.astype(jnp.bfloat16).reshape(tok_count, head_local * HDIM)
     row_count = residual.shape[0]
-    token_rows = lax.all_to_all(attended, "tp", split_axis=0, concat_axis=1, tiled=True)
+    token_rows = jnp.concatenate(
+        lax.all_to_all(jnp.stack(jnp.split(attended, lax.axis_size("tp"), axis=0)), "tp", 0, 0),
+        axis=1,
+    )
     projected = jnp.dot(
         token_rows,
         lax.all_gather(out_weight, "tp", axis=0, tiled=True),

time: 196 us -> 196 us (level)
  no operation moved by 1% of the time
where the time goes in v1:
time: 196 us; the launch traced here: 195 us
  waiting for transfers between devices  72.4 us (37%)
  blocking collectives  53.4 us (27%)
  local copies, waits for them, and re-layouts  19.8 us (10%)
  between operations  13.7 us (7%)
  starting transfers between devices  12.8 us (7%)
  matrix products  12.6 us (6%)
  other arithmetic  10.7 us (5%)
    all_to_all x1, blocking collectives, per_device(): lax.all_to_all(outgoing, ('sp', 'tp'), split_axis=0, concat_axis=0, tiled...  53.4 us
    all_to_all x1, waiting for transfers between devices, per_device(): lax.all_to_all(produced.reshape(arrived.shape), ('sp', 'tp'), split_axis=...  47.4 us
    all_gather x1, waiting for transfers between devices, per_device(): lax.all_gather(out_weight, 'tp', axis=0, tiled=True)  16.9 us
    all_to_all x1, waiting for transfers between devices, per_device(): lax.all_to_all(jnp.stack(jnp.split(attended, lax.axis_size('tp'), axis=0)...  7.38 us
    scatter x1, local copies, waits for them, and re-layouts, per_device(): outgoing = jnp.zeros((expert_count * capacity, width), jnp.bfloat16).at[s...  7.33 us
    dot_general x1, matrix products, per_device(): jnp.dot(hidden, down_weight[0], preferred_element_type=jnp.float32)  6.26 us
    gather x1, local copies, waits for them, and re-layouts, per_device(): returned.reshape(expert_count * capacity, width)[slot_index]  5.19 us
    all_to_all x1, starting transfers between devices, per_device(): lax.all_to_all(produced.reshape(arrived.shape), ('sp', 'tp'), split_axis=...  5.15 us
  transfers between devices with their start and end apart: 4, of which 3 were waited for; matrix products, arithmetic and copies ran while one was open for 4% of the time, Pallas kernels for 0%

profile of v1, /device:TPU:11, one launch (start us, length us, event | category | flops | bytes accessed | tf_op | source)
XLA Modules:
  0.0 195.3 jit_solution(17217919698374945270)
XLA Ops:
  6.5 0.0 copy-start
  6.5 0.0 copy-start.5
  6.5 0.0 copy-start.2
  6.5 0.0 all-gather.2.cloned.1.call-start
  6.5 0.7 all-gather.2.cloned.1.call-update
  7.3 0.0 copy-start.3
  7.3 0.0 slice-start
  7.3 0.9 bitcast_convert_fusion
  8.2 0.3 fusion.39
  8.5 0.7 slice_bitcast_fusion.4
  9.3 3.2 %collective-permute-start = (bf16[2,128,64]{1,2,0:T(8,128)(2,1)S(1)}, bf16[2,128,64]{1,2,0:T(8,128)(2,1)S(1)}, u32[]{:S(2)}, u32[]{:S(2)}) collective-permute-start(bf16[2,128,64]{1,2,0:T(8,128)(2,1)S(1)} %pad_maximum_fusion.1), channel_id=1, source_target_pairs={{0,4},{4,8},{8,12},{1,5},{5,9},{9,13},{2,6},{6,10},{10,14},{3,7},{... | collective-permute-start | bytes 98312 | tf_op jit(solution)/shard_map/ppermute | solution.py:15
  12.5 0.8 copy.25
  13.2 0.1 eq.29
  13.4 0.1 eq.25
  13.5 0.0 copy-done.2
  13.5 0.1 copy.21
  13.7 0.1 convert.12
  13.8 0.6 reduce-window.6
  14.3 0.2 slice_reduce_fusion
  14.6 0.1 fusion.43
  14.7 0.1 add_compare_fusion
  14.8 0.0 copy-done.5
  14.8 0.3 multiply_cosine_fusion
  15.2 0.2 broadcast_and_fusion
  15.4 0.1 subtract_convert_fusion
  15.5 0.0 copy-start.6
  15.5 0.0 copy-done.3
  15.5 0.0 slice-done
  15.6 0.1 copy.24
  15.7 0.1 mul.180
  15.8 0.0 collective-permute-done
  15.9 0.5 fusion.49
  16.4 0.0 copy-done.6
  16.4 0.1 broadcast_maximum_fusion
  16.5 0.3 fusion.7
  16.8 0.1 exponential_add_fusion
  16.9 0.5 fusion.14
  17.4 0.7 pad_maximum_fusion
  18.1 4.5 %all-to-all-start = ((bf16[4,128,256]{1,2,0:T(8,128)(2,1)}), bf16[4,128,256]{1,2,0:T(8,128)(2,1)S(1)}, u32[]{:S(2)}, u32[]{:S(2)}) async-start(bf16[4,128,256]{1,2,0:T(8,128)(2,1)} %pad_maximum_fusion), calls=%async_computation | async-start | bytes 524288 | tf_op jit(solution)/shard_map/all_to_all | solution.py:90
  22.6 7.4 %all-to-all-done = bf16[4,128,256]{1,2,0:T(8,128)(2,1)S(1)} async-done(((bf16[4,128,256]{1,2,0:T(8,128)(2,1)}), bf16[4,128,256]{1,2,0:T(8,128)(2,1)S(1)}, u32[]{:S(2)}, u32[]{:S(2)}) %all-to-all-start) | async-done | bytes 262176 | tf_op jit(solution)/shard_map/all_to_all | solution.py:90
  30.0 16.9 %all-gather.2.cloned.1.call-done = bf16[1024,2048]{1,0:T(8,128)(2,1)} async-done(((bf16[256,2048]{1,0:T(8,128)(2,1)}), bf16[1024,2048]{1,0:T(8,128)(2,1)}) %all-gather.2.cloned.1.call-update) | async-done | bytes 4194320 | tf_op jit(solution)/shard_map/all_gather | solution.py:95
  46.9 0.0 copy-start.4
  46.9 3.1 %multiply_reduce_fusion.1 = (f32[128]{0:T(128)S(1)}, f32[128,2048]{1,0:T(8,128)S(1)}) fusion(bf16[128,1024]{0,1:T(8,128)(2,1)S(1)} %bitcast.119, bf16[1024,2048]{1,0:T(8,128)(2,1)} %all-gather.2.cloned.1.call-done, bf16[128,2048]{1,0:T(8,128)(2,1)} %param.16), kind=kOutput, calls=%fused_computation.26 | convolution fusion | flops 538443648 | bytes 6029824 | tf_op jit(solution)/shard_map/dot_general | solution.py:93
  50.0 0.0 copy-done.4
  50.0 1.0 multiply_convert_fusion
  51.0 7.3 %scatter_custom_fusion = bf16[512,2048]{1,0:T(8,128)(2,1)} fusion(s32[256]{0:T(256)S(1)} %bitcast.126, bf16[128,2048]{1,0:T(8,128)(2,1)} %multiply_convert_fusion, s32[1024]{0:T(1024)S(1)} %pad_clamp_fusion.1, bf16[]{:T(256)} %constant.56.clone.1), kind=kCustom, calls=%fused_computation.22 | custom fusion | bytes 2097664 | tf_op jit(solution)/shard_map/scatter | solution.py:119
  58.3 0.0 copy-start.8
  58.3 53.4 %all_to_all.15 = bf16[16,32,2048]{2,1,0:T(8,128)(2,1)S(1)} all-to-all(bf16[16,32,2048]{2,1,0:T(8,128)(2,1)} %bitcast.115), channel_id=1, replica_groups=mesh['grp'=2,'sp'=4,'tp'=4] {'sp','tp'}, dimensions={0} | all-to-all | bytes 4194304 | tf_op jit(solution)/shard_map/all_to_all | solution.py:122
  111.6 0.0 copy-start.1
  111.6 1.3 copy-done.1
  113.0 0.0 copy-done.8
  113.0 2.2 %fusion.5 = f32[512,512]{1,0:T(8,128)} fusion(bf16[512,2048]{1,0:T(8,128)(2,1)S(1)} %bitcast.117, bf16[1,2048,512]{2,1,0:T(8,128)(2,1)S(1)} %copy-done.8), kind=kOutput, calls=%fused_computation.11 | convolution fusion | flops 1073741824 | bytes 5242880 | tf_op jit(solution)/shard_map/dot_general | solution.py:124
  115.2 0.0 copy-done
  115.2 6.3 %convolution_convert_fusion = bf16[512,2048]{1,0:T(8,128)(2,1)} fusion(bf16[1,512,2048]{2,1,0:T(8,128)(2,1)S(1)} %copy-done, bf16[512,2048]{1,0:T(8,128)(2,1)} %bitcast.118, bf16[1,2048,512]{2,1,0:T(8,128)(2,1)} %param.20, f32[512,512]{1,0:T(8,128)} %fusion.5), kind=kOutput, calls=%fused_computation.3 | convolution fusion | flops 2150105088 | bytes 9437184 | tf_op jit(solution)/shard_map/dot_general | solution.py:127
  121.4 0.0 copy-start.7
  121.4 5.2 %all-to-all-start.2 = ((bf16[16,32,2048]{2,1,0:T(8,128)(2,1)}), bf16[16,32,2048]{2,1,0:T(8,128)(2,1)}, u32[]{:S(2)}, u32[]{:S(2)}) async-start(bf16[16,32,2048]{2,1,0:T(8,128)(2,1)} %bitcast.116), calls=%async_computation.2 | async-start | bytes 4194304 | tf_op jit(solution)/shard_map/all_to_all | solution.py:130
  126.6 0.0 copy-done.7
  126.6 0.1 copy.28
  126.7 47.4 %all-to-all-done.2 = bf16[16,32,2048]{2,1,0:T(8,128)(2,1)} async-done(((bf16[16,32,2048]{2,1,0:T(8,128)(2,1)}), bf16[16,32,2048]{2,1,0:T(8,128)(2,1)}, u32[]{:S(2)}, u32[]{:S(2)}) %all-to-all-start.2) | async-done | bytes 2097184 | tf_op jit(solution)/shard_map/all_to_all | solution.py:130
  174.1 5.2 %gather_fusion = bf16[256,2048]{1,0:T(8,128)(2,1)} fusion(bf16[512,2048]{1,0:T(8,128)(2,1)} %bitcast.37, s32[1024]{0:T(1024)S(1)} %pad_clamp_fusion), kind=kCustom, calls=%fused_computation.1 | custom fusion | bytes 2098176 | tf_op jit(solution)/shard_map/gather | solution.py:133
  179.3 3.4 %reshape.403 = f32[128,2,2048]{2,1,0:T(2,128)} reshape(bf16[256,2048]{1,0:T(8,128)(2,1)} %gather_fusion) | data formatting | bytes 3145728 | tf_op jit(solution)/shard_map/convert_element_type | solution.py:133
  182.7 4.8 %multiply_reduce_fusion = f32[128,2048]{1,0:T(8,128)S(1)} fusion(f32[128,2,2048]{2,1,0:T(2,128)} %reshape.403, f32[128,2]{1,0:T(8,128)S(1)} %copy.28), kind=kLoop, calls=%fused_computation.13 | loop fusion | flops 786432 | bytes 3146752 | tf_op jit(solution)/shard_map/reduce_sum | solution.py:135
  187.5 0.9 add_convert_fusion
  (25 shorter events, 0.3 us)
Async XLA Ops:
  6.5 108.6 %copy-start = (bf16[1,512,2048]{2,1,0:T(8,128)(2,1)S(1)}, bf16[1,512,2048]{2,1,0:T(8,128)(2,1)}, u32[]{:S(2)}) copy-start(bf16[1,512,2048]{2,1,0:T(8,128)(2,1)} %param.21) | copy-start | bytes 6291460
  6.5 8.2 %copy-start.5 = (s32[128,2]{0,1:T(2,128)S(1)}, s32[128,2]{0,1:T(2,128)}, u32[]{:S(2)}) copy-start(s32[128,2]{0,1:T(2,128)} %param.22) | copy-start | bytes 3076
  6.5 7.0 %copy-start.2 = (bf16[512,256]{1,0:T(8,128)(2,1)S(1)}, bf16[512,256]{1,0:T(8,128)(2,1)}, u32[]{:S(2)}) copy-start(bf16[512,256]{1,0:T(8,128)(2,1)} %param.12) | copy-start | bytes 786436
  6.5 40.3 %all-gather.2.cloned.1.call-start = ((), (), s32[]{:S(2)}) async-start(), calls=%async_computation.3 | async-start | bytes 5242880 | tf_op jit(solution)/shard_map/all_gather | solution.py:95
  7.3 8.2 %copy-start.3 = (bf16[512,64]{0,1:T(8,128)(2,1)S(1)}, bf16[512,64]{0,1:T(8,128)(2,1)}, u32[]{:S(2)}) copy-start(bf16[512,64]{0,1:T(8,128)(2,1)} %param.14) | copy-start | bytes 196612
  7.3 8.2 %slice-start = ((bf16[512,64]{0,1:T(8,128)(2,1)}), bf16[384,64]{0,1:T(8,128)(2,1)S(1)}, s32[]{:S(2)}) async-start(bf16[512,64]{0,1:T(8,128)(2,1)} %param.14), calls=%async_computation.4 | async-start | bytes 98304 | tf_op jit(solution)/shard_map/slice | solution.py:65
  9.3 6.6 %collective-permute-start = (bf16[2,128,64]{1,2,0:T(8,128)(2,1)S(1)}, bf16[2,128,64]{1,2,0:T(8,128)(2,1)S(1)}, u32[]{:S(2)}, u32[]{:S(2)}) collective-permute-start(bf16[2,128,64]{1,2,0:T(8,128)(2,1)S(1)} %pad_maximum_fusion.1), channel_id=1, source_target_pairs={{0,4},{4,8},{8,12},{1,5},{5,9},{9,13},{2,6},{6,10},{10,14},{3,7},{... | collective-permute-start | bytes 98312 | tf_op jit(solution)/shard_map/ppermute | solution.py:15
  15.5 0.9 copy-start.6
  18.1 11.9 %all-to-all-start = ((bf16[4,128,256]{1,2,0:T(8,128)(2,1)}), bf16[4,128,256]{1,2,0:T(8,128)(2,1)S(1)}, u32[]{:S(2)}, u32[]{:S(2)}) async-start(bf16[4,128,256]{1,2,0:T(8,128)(2,1)} %pad_maximum_fusion), calls=%async_computation | async-start | bytes 524288 | tf_op jit(solution)/shard_map/all_to_all | solution.py:90
  46.9 3.2 %copy-start.4 = (f32[2048]{0:T(1024)S(1)}, f32[2048]{0:T(1024)}, u32[]{:S(2)}) copy-start(f32[2048]{0:T(1024)} %param.18) | copy-start | bytes 24580
  58.3 54.7 %copy-start.8 = (bf16[1,2048,512]{2,1,0:T(8,128)(2,1)S(1)}, bf16[1,2048,512]{2,1,0:T(8,128)(2,1)}, u32[]{:S(2)}) copy-start(bf16[1,2048,512]{2,1,0:T(8,128)(2,1)} %param.19) | copy-start | bytes 6291460
  111.6 1.3 copy-start.1
  121.4 5.2 %copy-start.7 = (f32[128,2]{0,1:T(2,128)S(1)}, f32[128,2]{0,1:T(2,128)}, u32[]{:S(2)}) copy-start(f32[128,2]{0,1:T(2,128)} %param.23) | copy-start | bytes 3076
  121.4 52.7 %all-to-all-start.2 = ((bf16[16,32,2048]{2,1,0:T(8,128)(2,1)}), bf16[16,32,2048]{2,1,0:T(8,128)(2,1)}, u32[]{:S(2)}, u32[]{:S(2)}) async-start(bf16[16,32,2048]{2,1,0:T(8,128)(2,1)} %bitcast.116), calls=%async_computation.2 | async-start | bytes 4194304 | tf_op jit(solution)/shard_map/all_to_all | solution.py:130
Sparse Core Ops, SparseCore 0:
  8.9 37.9 all-gather.1
